TPU v7x, 32 devices: a whole 2x2x4 slice. The times are simulated.
32 devices in a mesh: ep: 8 (over z, core), tp: 4 (over y, x).
Axes of the slice: x: 2, y: 2, z: 4, core: 2. Of those that a mesh axis runs over, the one named last changes fastest.
Arguments:
- branch_in: bfloat16 [8192, 512], P(('ep', 'tp')), may hold values from -6 to 6
- pool_weight: bfloat16 [4, 128, 128], replicated, may hold values from -0.5 to 0.5
- group_gain: float32 [512], replicated, may hold values from 0.1 to 1.9
- out_weight: bfloat16 [512, 2048], P(None, 'tp'), may hold values from -0.25 to 0.25
- out_gain: float32 [2048], replicated, may hold values from 0.1 to 1.9
- ffn_input: bfloat16 [1024, 2048], P('ep'), may hold values from -6 to 6
- ffn_gain: float32 [2048], replicated, may hold values from 0.1 to 1.9
- routes: int32 [1024, 4], P('ep'), may hold values from 0 to 7, all different within a row; in each aligned block of 128 rows (0 to 127, 128 to 255, ...) at most 128 rows name the same one
- route_weight: float32 [1024, 4], P('ep'), may hold values from 0.2 to 2
- gate_weight: bfloat16 [8, 2048, 4096], P('ep', None, 'tp'), may hold values from -0.375 to 0.375
- up_weight: bfloat16 [8, 2048, 4096], P('ep', None, 'tp'), may hold values from -0.375 to 0.375
- down_weight: bfloat16 [8, 4096, 2048], P('ep', 'tp'), may hold values from -0.0078125 to 0.0078125
Outputs:
- mixer_out: bfloat16 [8192, 2048], P(('ep', 'tp'))
- expert_out: bfloat16 [1024, 2048], P('ep', 'tp')
Inputs may be any that keep to these rules, and one draw needn't show every extreme that they name: `routes`: each row names 4 different experts. Among the 128 rows of one index of ep no expert is named by more than 128 rows, and in some such block one expert is named by exactly 128.
All inputs are finite; a program needn't handle non-finite values.
Results may differ from a plain program's by a relative error of at most 0.017.
Values may be sent and summed in bfloat16 or wider, within the bound.
A program may use at most 64 MiB of HBM per device.

v0:
```python
import jax
import jax.numpy as jnp
from jax import lax
from jax.sharding import PartitionSpec as P

pool_windows = (2, 4, 8, 16)
rim_rows = 15
norm_eps = 1e-06
clamp_limit = 7.0
sigmoid_slope = 1.702


def shifted_2(block, axis, distance):
    devices = range(lax.axis_size(axis))
    route = [(i - distance, i) for i in devices if i - distance in devices]
    return lax.ppermute(block, axis, route)


def rms_scale(values, gain):
    return values * lax.rsqrt(jnp.mean(values * values, axis=-1, keepdims=True) + norm_eps) * gain


def slot_tables(route_block, expert_count, capacity):
    row_count, top_count = route_block.shape
    flat_experts = route_block.reshape(-1)
    one_hot = (flat_experts[:, None] == jnp.arange(expert_count, dtype=jnp.int32)[None, :]).astype(
        jnp.int32
    )
    earlier = jnp.cumsum(one_hot, axis=0) - one_hot
    slot_index = jnp.sum(earlier * one_hot, axis=1)
    flat_slots = slot_index * expert_count + flat_experts
    owner_rows = jnp.full((capacity * expert_count,), row_count, jnp.int32)
    owner_rows = owner_rows.at[flat_slots].set(
        jnp.arange(row_count * top_count, dtype=jnp.int32) // top_count
    )
    return (flat_slots, owner_rows)


def pool_branch(branch_in, pool_weight, group_gain, out_weight, out_gain):
    row_count, width = branch_in.shape
    group_chans = width // len(pool_windows)
    rim = shifted_2(branch_in[row_count - rim_rows :], ("ep", "tp"), 1)
    widened = jnp.concatenate([rim, branch_in], axis=0).astype(jnp.float32)
    first_row = (lax.axis_index("ep") * lax.axis_size("tp") + lax.axis_index("tp")) * row_count
    positions = first_row + jnp.arange(row_count, dtype=jnp.int32)
    window = jnp.repeat(jnp.array(pool_windows, jnp.int32), group_chans)
    summed = jnp.zeros((row_count, width), jnp.float32)
    for offset_back in range(rim_rows + 1):
        shifted = widened[rim_rows - offset_back : rim_rows - offset_back + row_count]
        summed = summed + jnp.where(window[None, :] > offset_back, shifted, jnp.float32(0.0))
    counts = jnp.minimum(window[None, :], positions[:, None] + 1).astype(jnp.float32)
    pooled = (summed / counts - widened[rim_rows:]).astype(jnp.bfloat16)
    mixed_parts = []
    for group_index in range(len(pool_windows)):
        lower = group_index * group_chans
        mixed_parts.append(
            jnp.dot(
                pooled[:, lower : lower + group_chans],
                pool_weight[group_index],
                preferred_element_type=jnp.float32,
            )
        )
    group_mix = jnp.concatenate(mixed_parts, axis=1)
    mixed_rows = rms_scale(group_mix, group_gain).astype(jnp.bfloat16)
    projected = jnp.dot(
        mixed_rows,
        lax.all_gather(out_weight, "tp", axis=1, tiled=True),
        preferred_element_type=jnp.float32,
    )
    return rms_scale(projected, out_gain).astype(jnp.bfloat16)


def expert_hidden(slot_rows, gate_local, up_local):
    gate_pre = jnp.einsum("sed,df->sef", slot_rows, gate_local, preferred_element_type=jnp.float32)
    up_pre = jnp.einsum("sed,df->sef", slot_rows, up_local, preferred_element_type=jnp.float32)
    gate_pre = jnp.minimum(gate_pre, clamp_limit)
    up_pre = jnp.clip(up_pre, -clamp_limit, clamp_limit)
    return ((up_pre + 1.0) * gate_pre * jax.nn.sigmoid(sigmoid_slope * gate_pre)).astype(
        jnp.bfloat16
    )


def send_home(hidden, down_local):
    partial_sum = jnp.einsum("sef,fd->sed", hidden, down_local, preferred_element_type=jnp.float32)
    partial_sum = partial_sum.astype(jnp.bfloat16).astype(jnp.float32)
    summed = lax.psum_scatter(
        partial_sum.astype(jnp.bfloat16), "tp", scatter_dimension=2, tiled=True
    )
    return lax.all_to_all(summed, "ep", split_axis=1, concat_axis=1, tiled=True)


def per_device(
    branch_in,
    pool_weight,
    group_gain,
    out_weight,
    out_gain,
    ffn_input,
    ffn_gain,
    routes,
    route_weight,
    gate_weight,
    up_weight,
    down_weight,
):
    mixer_out = pool_branch(branch_in, pool_weight, group_gain, out_weight, out_gain)
    normed_rows = rms_scale(ffn_input.astype(jnp.float32), ffn_gain).astype(jnp.bfloat16)
    row_count, model_width = normed_rows.shape
    top_count = routes.shape[1]
    expert_count = lax.axis_size("ep")
    capacity = 2 * row_count * top_count // expert_count
    flat_slots, owner_rows = slot_tables(routes, expert_count, capacity)
    padded = jnp.concatenate([normed_rows, jnp.zeros((1, model_width), jnp.bfloat16)], axis=0)
    slot_rows = padded[owner_rows].reshape(capacity, expert_count, model_width)
    gate_local = gate_weight[0]
    up_local = up_weight[0]
    down_local = down_weight[0]
    share = capacity // lax.axis_size("tp")
    my_share = lax.dynamic_slice_in_dim(slot_rows, lax.axis_index("tp") * share, share, 0)
    arrived = lax.all_to_all(my_share, "ep", split_axis=1, concat_axis=1, tiled=True)
    hidden = expert_hidden(lax.all_gather(arrived, "tp", axis=0, tiled=True), gate_local, up_local)
    returned = send_home(hidden, down_local)
    column_count = returned.shape[2]
    picked = returned.reshape(capacity * expert_count, column_count)[flat_slots]
    picked = picked.reshape(row_count, top_count, column_count).astype(jnp.float32)
    expert_out = jnp.sum(picked * route_weight[:, :, None], axis=1).astype(jnp.bfloat16)
    return (mixer_out, expert_out)


def solution(mesh):
    in_specs = (
        P(("ep", "tp"), None),
        P(),
        P(),
        P(None, "tp"),
        P(),
        P("ep", None),
        P(),
        P("ep", None),
        P("ep", None),
        P("ep", None, "tp"),
        P("ep", None, "tp"),
        P("ep", "tp", None),
    )
    out_specs = (P(("ep", "tp"), None), P("ep", "tp"))
    return jax.shard_map(
        per_device, mesh=mesh, in_specs=in_specs, out_specs=out_specs, check_vma=False
    )
```

profile of v0, /device:TPU:0, one launch (start us, length us, event | category | flops | bytes accessed | tf_op | source)
XLA Modules:
  0.0 230.9 jit_solution(12385050998380482686)
XLA Ops:
  7.2 0.0 all-gather.5.cloned.1.call-start
  7.2 0.8 copy.16
  8.0 0.1 eq.29
  8.1 0.1 eq.25
  8.2 0.1 reshape.209
  8.4 1.1 reduce-window.6
  9.5 0.2 slice_reduce_fusion
  9.8 0.1 fusion.52
  9.9 2.4 %scatter_custom_fusion = s32[1024]{0:T(1024)S(1)} fusion(s32[512]{0:T(512)S(1)} %bitcast.66, s32[512]{0:T(512)S(1)} %add_select_fusion, s32[]{:T(128)} %constant.34.clone.1), kind=kCustom, calls=%fused_computation.109 | custom fusion | bytes 4100 | tf_op jit(solution)/shard_map/scatter | solution.py:33
  12.3 1.2 fusion.11
  13.6 1.2 fusion.13
  14.9 6.0 %gather_fusion = bf16[1024,2048]{1,0:T(8,128)(2,1)} fusion(bf16[129,2048]{1,0:T(8,128)(2,1)S(1)} %concatenate.11, s32[1024]{0:T(1024)S(1)} %fusion.54), kind=kCustom, calls=%fused_computation | custom fusion | bytes 8392704 | tf_op jit(solution)/shard_map/gather | solution.py:114
  20.9 1.3 constant_dynamic-slice_fusion
  22.2 0.6 copy.22
  22.8 32.8 %all_to_all.10 = bf16[32,8,2048]{2,0,1:T(8,128)(2,1)} all-to-all(bf16[32,8,2048]{2,0,1:T(8,128)(2,1)S(1)} %copy.22), channel_id=1, replica_groups=mesh['ep'=8,'tp'=4] {'ep'}, dimensions={1} | all-to-all | bytes 2097152 | tf_op jit(solution)/shard_map/all_to_all | solution.py:120
  55.6 0.0 all-gather.5.cloned.1.call-update
  55.6 0.0 reduce-scatter.2.cloned.1.call-start
  55.7 51.6 %all-gather.5.cloned.1.call-done = bf16[128,8,2048]{2,0,1:T(8,128)(2,1)} async-done(((bf16[32,8,2048]{2,0,1:T(8,128)(2,1)}), bf16[128,8,2048]{2,0,1:T(8,128)(2,1)}) %all-gather.5.cloned.1.call-update) | async-done | bytes 4194320 | tf_op jit(solution)/shard_map/all_gather | solution.py:121
  107.3 7.6 %fusion.2 = f32[128,8,1024]{2,0,1:T(8,128)S(1)} fusion(bf16[128,8,2048]{2,0,1:T(8,128)(2,1)} %all-gather.5.cloned.1.call-done, bf16[1,2048,1024]{2,1,0:T(8,128)(2,1)} %param.22), kind=kOutput, calls=%fused_computation.5 | convolution fusion | flops 4294967296 | bytes 12582912 | tf_op jit(solution)/shard_map/sed,df->sef/dot_general | solution.py:74
  115.0 5.7 %multiply_convert_fusion = bf16[128,8,1024]{2,0,1:T(8,128)(2,1)S(1)} fusion(f32[128,8,1024]{2,0,1:T(8,128)S(1)} %fusion.2, bf16[128,8,2048]{2,0,1:T(8,128)(2,1)S(1)} %copy-done.8, bf16[1,2048,1024]{2,1,0:T(8,128)(2,1)S(1)} %copy-done.6), kind=kOutput, calls=%fused_computation.9 | convolution fusion | flops 4305453056 | bytes 14680064 | tf_op jit(solution)/shard_map/sed,df->sef/dot_general | solution.py:75
  120.6 6.1 %fusion.6 = bf16[128,8,2048]{2,0,1:T(8,128)(2,1)} fusion(bf16[128,8,1024]{2,0,1:T(8,128)(2,1)S(1)} %multiply_convert_fusion, bf16[1,1024,2048]{2,1,0:T(8,128)(2,1)S(1)} %copy-done.7), kind=kOutput, calls=%fused_computation.10 | convolution fusion | flops 4297064448 | bytes 10485760 | tf_op jit(solution)/shard_map/sef,fd->sed/dot_general | solution.py:84
  126.7 0.0 reduce-scatter.2.cloned.1.call-update
  126.7 0.0 all-gather.3.cloned.1.call-start
  126.8 0.7 all-gather.3.cloned.1.call-update
  127.5 0.2 copy-done
  127.7 3.4 %collective-permute-start = (bf16[15,512]{1,0:T(8,128)(2,1)S(1)}, bf16[15,512]{1,0:T(8,128)(2,1)S(1)}, u32[]{:S(2)}, u32[]{:S(2)}) collective-permute-start(bf16[15,512]{1,0:T(8,128)(2,1)S(1)} %slice.82), channel_id=1, source_target_pairs={{0,1},{1,2},{2,3},{3,4},{4,5},{5,6},{6,7},{7,8},{8,9},{9,10},{10,1... | collective-permute-start | bytes 46088 | tf_op jit(solution)/shard_map/ppermute | solution.py:16
  131.1 0.1 broadcast_bitcast_fusion
  131.2 0.1 bitcast_compare_fusion.15
  131.3 0.1 copy.21
  131.4 1.1 collective-permute-done
  132.5 0.1 maximum_convert_fusion
  132.6 0.0 copy-start.1
  132.6 1.1 fusion.31
  133.7 0.0 copy-start.2
  133.8 0.2 fusion.35
  134.0 45.5 %reduce-scatter.2.cloned.1.call-done = bf16[128,8,512]{2,0,1:T(8,128)(2,1)} async-done(((bf16[128,8,2048]{2,0,1:T(8,128)(2,1)}), bf16[128,8,512]{2,0,1:T(8,128)(2,1)}) %reduce-scatter.2.cloned.1.call-update) | async-done | bytes 1048592 | tf_op jit(solution)/shard_map/reduce_scatter | solution.py:86
  179.5 4.6 %all-to-all-start.1 = ((bf16[128,8,512]{2,0,1:T(8,128)(2,1)}), bf16[128,8,512]{2,0,1:T(8,128)(2,1)S(1)}, u32[]{:S(2)}, u32[]{:S(2)}) async-start(bf16[128,8,512]{2,0,1:T(8,128)(2,1)} %reduce-scatter.2.cloned.1.call-done), calls=%async_computation.2 | async-start | bytes 2097152 | tf_op jit(solution)/shard_map/all_to_all | solution.py:89
  184.1 0.2 fusion.37
  184.3 0.2 fusion.39
  184.5 0.2 fusion.41
  184.8 0.1 multiply_reduce_fusion.2
  184.8 31.5 %all-gather.3.cloned.1.call-done = bf16[512,2048]{1,0:T(8,128)(2,1)} async-done(((bf16[512,512]{1,0:T(8,128)(2,1)}), bf16[512,2048]{1,0:T(8,128)(2,1)}) %all-gather.3.cloned.1.call-update) | async-done | bytes 2097168 | tf_op jit(solution)/shard_map/all_gather | solution.py:67
  216.4 2.5 %multiply_reduce_fusion = (f32[256]{0:T(256)S(1)}, f32[256,2048]{1,0:T(8,128)S(1)}) fusion(bf16[512,2048]{1,0:T(8,128)(2,1)} %all-gather.3.cloned.1.call-done, f32[256,128]{0,1:T(8,128)S(1)} %fusion.35, f32[256,128]{0,1:T(8,128)S(1)} %fusion.37, f32[256,128]{0,1:T(8,128)S(1)} %fusion.39, f32[256,128]{0,1:T(8,128)S(1)} %fusion.41, f32[512]{0:T(512)S(1)} %copy-done.3, ...), kind=kOutput, calls=%fused_computation.12 | convolution fusion | flops 538705664 | bytes 4722688 | tf_op jit(solution)/shard_map/dot_general | solution.py:65
  218.9 1.2 multiply_convert_fusion.1
  220.2 0.6 copy.24
  220.7 2.0 gather_fusion.1
  222.7 0.3 reshape.212
  223.0 1.4 multiply_reduce_fusion.1
  (30 shorter events, 0.2 us)
Async XLA Ops:
  7.2 100.1 %all-gather.5.cloned.1.call-start = ((), (), s32[]{:S(2)}) async-start(), calls=%async_computation.4 | async-start | bytes 5242880 | tf_op jit(solution)/shard_map/all_gather | solution.py:121
  55.6 123.9 %reduce-scatter.2.cloned.1.call-start = ((), (), s32[]{:S(2)}) async-start(), calls=%async_computation.5 | async-start | bytes 5242880 | tf_op jit(solution)/shard_map/reduce_scatter | solution.py:86
  107.3 7.7 %copy-start.6 = (bf16[1,2048,1024]{2,1,0:T(8,128)(2,1)S(1)}, bf16[1,2048,1024]{2,1,0:T(8,128)(2,1)}, u32[]{:S(2)}) copy-start(bf16[1,2048,1024]{2,1,0:T(8,128)(2,1)} %param.23) | copy-start | bytes 12582916
  107.3 7.7 %copy-start.8 = (bf16[128,8,2048]{2,0,1:T(8,128)(2,1)S(1)}, bf16[128,8,2048]{2,0,1:T(8,128)(2,1)}, u32[]{:S(2)}) copy-start(bf16[128,8,2048]{2,0,1:T(8,128)(2,1)} %all-gather.5.cloned.1.call-done) | copy-start | bytes 12582916
  115.0 5.7 %copy-start.7 = (bf16[1,1024,2048]{2,1,0:T(8,128)(2,1)S(1)}, bf16[1,1024,2048]{2,1,0:T(8,128)(2,1)}, u32[]{:S(2)}) copy-start(bf16[1,1024,2048]{2,1,0:T(8,128)(2,1)} %param.24) | copy-start | bytes 12582916
  126.7 0.9 copy-start
  126.7 4.4 %copy-start.5 = (s32[4]{0:T(128)S(1)}, s32[4]{0:T(128)}, u32[]{:S(2)}) copy-start(s32[4]{0:T(128)} %constant.101.clone) | copy-start | bytes 52
  126.7 4.5 %copy-start.4 = (f32[128,4]{0,1:T(4,128)S(1)}, f32[128,4]{0,1:T(4,128)}, u32[]{:S(2)}) copy-start(f32[128,4]{0,1:T(4,128)} %param.21) | copy-start | bytes 6148
  126.7 89.6 %all-gather.3.cloned.1.call-start = ((), (), s32[]{:S(2)}) async-start(), calls=%async_computation.3 | async-start | bytes 2621440 | tf_op jit(solution)/shard_map/all_gather | solution.py:67
  127.7 4.8 %collective-permute-start = (bf16[15,512]{1,0:T(8,128)(2,1)S(1)}, bf16[15,512]{1,0:T(8,128)(2,1)S(1)}, u32[]{:S(2)}, u32[]{:S(2)}) collective-permute-start(bf16[15,512]{1,0:T(8,128)(2,1)S(1)} %slice.82), channel_id=1, source_target_pairs={{0,1},{1,2},{2,3},{3,4},{4,5},{5,6},{6,7},{7,8},{8,9},{9,10},{10,1... | collective-permute-start | bytes 46088 | tf_op jit(solution)/shard_map/ppermute | solution.py:16
  132.6 1.2 copy-start.1
  132.6 83.8 %copy-start.3 = (f32[512]{0:T(512)S(1)}, f32[512]{0:T(512)}, u32[]{:S(2)}) copy-start(f32[512]{0:T(512)} %param.15) | copy-start | bytes 6148
  133.7 85.2 %copy-start.2 = (f32[2048]{0:T(1024)S(1)}, f32[2048]{0:T(1024)}, u32[]{:S(2)}) copy-start(f32[2048]{0:T(1024)} %param.17) | copy-start | bytes 24580
  179.5 40.7 %all-to-all-start.1 = ((bf16[128,8,512]{2,0,1:T(8,128)(2,1)}), bf16[128,8,512]{2,0,1:T(8,128)(2,1)S(1)}, u32[]{:S(2)}, u32[]{:S(2)}) async-start(bf16[128,8,512]{2,0,1:T(8,128)(2,1)} %reduce-scatter.2.cloned.1.call-done), calls=%async_computation.2 | async-start | bytes 2097152 | tf_op jit(solution)/shard_map/all_to_all | solution.py:89
Sparse Core Ops, SparseCore 0:
  55.7 51.4 all-gather.4
  126.9 52.5 reduce-scatter.1
  181.3 35.0 all-gather.2
where the time goes:
time: 231 us
  waiting for transfers between devices  130 us (56%)
  blocking collectives  32.8 us (14%)
  matrix products  22.7 us (10%)
  local copies, waits for them, and re-layouts  15 us (6%)
  between operations  14 us (6%)
  starting transfers between devices  8.11 us (4%)
  other arithmetic  7.78 us (3%)
    all_gather x1, waiting for transfers between devices, per_device(): lax.all_gather(arrived, 'tp', axis=0, tiled=True)  51.6 us
    reduce_scatter x1, waiting for transfers between devices, send_home(): lax.psum_scatter(partial_sum.astype(jnp.bfloat16), 'tp', scatter_dimensio...  45.5 us
    all_to_all x1, blocking collectives, per_device(): lax.all_to_all(my_share, 'ep', split_axis=1, concat_axis=1, tiled=True)  32.8 us
    all_gather x1, waiting for transfers between devices, pool_branch(): lax.all_gather(out_weight, 'tp', axis=1, tiled=True)  31.5 us
    dot_general x1, matrix products, expert_hidden(): jnp.einsum('sed,df->sef', slot_rows, gate_local, preferred_element_type=j...  7.64 us
    dot_general x1, matrix products, send_home(): jnp.einsum('sef,fd->sed', hidden, down_local, preferred_element_type=jnp....  6.07 us
    gather x1, local copies, waits for them, and re-layouts, per_device(): slot_rows = padded[owner_rows].reshape(capacity, expert_count, model_width)  6.02 us
    dot_general x1, matrix products, expert_hidden(): jnp.einsum('sed,df->sef', slot_rows, up_local, preferred_element_type=jnp...  5.65 us
  transfers between devices with their start and end apart: 5, of which 4 were waited for; matrix products, arithmetic and copies ran while one was open for 3% of the time, Pallas kernels for 0%

commit v1 on v0

v1 whole, which is shorter than its diff:
```python
import functools
import jax
import jax.numpy as jnp
from jax import lax
from jax.experimental import pallas as pl
from jax.experimental.pallas import tpu as pltpu
from jax.sharding import PartitionSpec as P

pool_windows = (2, 4, 8, 16)
rim_rows = 16
norm_eps = 1e-06
clamp_limit = 7.0
sigmoid_slope = 1.702
MESH = pl.DeviceIdType.MESH
f32 = jnp.float32
bf16 = jnp.bfloat16


def rms_scale(values, gain):
    return values * lax.rsqrt(jnp.mean(values * values, axis=-1, keepdims=True) + norm_eps) * gain


def kernel(
    n_ep, n_tp,
    branch, pool_w, group_gain, out_w, out_gain, x_own, ffn_gain, w_own, gate_h, up_h, down_h,
    mixer_out, expert_out,
    gate, up, down, xg, wg, rim, ow, xn, hid, mixed, proj,
    pown, psend, precv, tsend, trecv, fsend, frecv, facc,
    local_sem, s_z, r_z, s_x, r_x, s_p, r_p, s_w, r_w, s_rim, r_rim,
    s_ow, r_ow, s_owp, r_owp, s_ps, r_ps, s_t, r_t, s_f, r_f,
):
    e = lax.axis_index("ep")
    j = lax.axis_index("tp")
    nz = n_ep // 2
    z = e // 2
    c = e % 2
    rows, width = x_own.shape
    cols = width // n_tp
    mate = z * 2 + (1 - c)
    last = (j == n_tp - 1).astype(jnp.int32)
    first = (j == 0).astype(jnp.int32)
    nxt = ((e + last) % n_ep, (j + 1) % n_tp)
    prv = ((e - first + n_ep) % n_ep, (j - 1 + n_tp) % n_tp)

    def colsl(q):
        return pl.ds(pl.multiple_of(q * cols, cols), cols)

    def remote(src, dst, ssem, rsem, ep, tp):
        return pltpu.make_async_remote_copy(
            src_ref=src, dst_ref=dst, send_sem=ssem, recv_sem=rsem,
            device_id=(ep, tp), device_id_type=MESH,
        )

    def ep_at(d):
        return (z + d) % nz * 2 + c

    def src_ep(d):
        return (z - d + nz) % nz * 2 + c

    def src_mate(d):
        return (z - d + nz) % nz * 2 + (1 - c)

    def tp_at(t):
        return (j + t) % n_tp

    loads = [
        pltpu.make_async_copy(gate_h.at[0], gate, local_sem.at[0]),
        pltpu.make_async_copy(up_h.at[0], up, local_sem.at[1]),
        pltpu.make_async_copy(down_h.at[0], down, local_sem.at[2]),
    ]
    own_copy = pltpu.make_async_copy(x_own, xg.at[e], local_sem.at[3])
    own_w = pltpu.make_async_copy(w_own, wg.at[e], local_sem.at[4])
    own_ow = pltpu.make_async_copy(out_w, ow.at[j], local_sem.at[5])
    own_copy.start()
    own_w.start()
    own_ow.start()
    for load in loads:
        load.start()

    barrier = pltpu.get_barrier_semaphore()
    for d in range(1, n_ep):
        pl.semaphore_signal(barrier, inc=1, device_id=((e + d) % n_ep, j), device_id_type=MESH)
    for t in range(1, n_tp):
        pl.semaphore_signal(barrier, inc=1, device_id=(e, tp_at(t)), device_id_type=MESH)
    pl.semaphore_signal(barrier, inc=1, device_id=nxt, device_id_type=MESH)
    pl.semaphore_signal(barrier, inc=1, device_id=prv, device_id_type=MESH)
    pl.semaphore_wait(barrier, n_ep - 1 + n_tp - 1 + 2)

    def z_copy(d):
        return remote(
            x_own.at[:, colsl(j)], xg.at[e, :, colsl(j)], s_z.at[d], r_z.at[d], ep_at(d), j
        )

    def z_arrival(d):
        view = xg.at[src_ep(d), :, colsl(j)]
        return remote(view, view, s_z.at[d], r_z.at[d], ep_at(d), j)

    def x_copy(d, t):
        view = xg.at[src_ep(d), :, colsl(j)]
        return remote(view, view, s_x.at[d, t], r_x.at[d, t], e, tp_at(t))

    def x_arrival(d, t):
        view = xg.at[src_ep(d), :, colsl(tp_at(n_tp - t))]
        return remote(view, view, s_x.at[d, t], r_x.at[d, t], e, tp_at(t))

    def p_copy(d):
        view = xg.at[src_ep(d)]
        return remote(view, view, s_p.at[d], r_p.at[d], mate, j)

    def p_arrival(d):
        view = xg.at[src_mate(d)]
        return remote(view, view, s_p.at[d], r_p.at[d], mate, j)

    own_p = remote(x_own, xg.at[e], s_p.at[0], r_p.at[0], mate, j)
    half = out_w.shape[0] // 2
    my_half = pl.ds(pl.multiple_of(c * half, half), half)
    mate_half = pl.ds(pl.multiple_of((1 - c) * half, half), half)

    def w_copy(d):
        return remote(w_own, wg.at[e], s_w.at[d], r_w.at[d], (e + d) % n_ep, j)

    def w_arrival(d):
        return remote(w_own, wg.at[(e - d + n_ep) % n_ep], s_w.at[d], r_w.at[d], (e + d) % n_ep, j)

    def ow_copy(t):
        return remote(
            out_w.at[my_half], ow.at[j, my_half], s_ow.at[t], r_ow.at[t], e, tp_at(t)
        )

    def ow_arrival(t):
        view = ow.at[tp_at(n_tp - t), my_half]
        return remote(view, view, s_ow.at[t], r_ow.at[t], e, tp_at(t))

    def owp_copy(t):
        view = ow.at[tp_at(n_tp - t), my_half]
        return remote(view, view, s_owp.at[t], r_owp.at[t], mate, j)

    def owp_arrival(t):
        view = ow.at[tp_at(n_tp - t), mate_half]
        return remote(view, view, s_owp.at[t], r_owp.at[t], mate, j)

    rim_copy = remote(
        branch.at[pl.ds(branch.shape[0] - rim_rows, rim_rows)], rim, s_rim, r_rim, nxt[0], nxt[1]
    )

    for d in range(1, nz):
        z_copy(d).start()
    own_p.start()
    rim_copy.start()
    for d in range(1, n_ep):
        w_copy(d).start()
    for t in range(1, n_tp):
        ow_copy(t).start()

    rim_copy.wait_recv()
    branch_rows = branch.shape[0]
    chans = branch.shape[1] // len(pool_windows)
    first_row = (e * n_tp + j) * branch_rows
    positions = first_row + lax.broadcasted_iota(jnp.int32, (branch_rows, 1), 0)
    total = jnp.zeros((branch_rows, 1), f32)
    for g, window in enumerate(pool_windows):
        lanes = slice(g * chans, (g + 1) * chans)
        here = branch[:, lanes].astype(f32)
        edge = jnp.where(first_row == 0, 0.0, rim[:, lanes].astype(f32))
        wide = jnp.concatenate([edge, here], axis=0)
        reach = 1
        while reach < window:
            wide = wide + pltpu.roll(wide, reach, 0)
            reach *= 2
        counts = jnp.minimum(window, positions + 1).astype(f32)
        pooled = (wide[rim_rows:] / counts - here).astype(bf16)
        part = jnp.dot(pooled, pool_w[g], preferred_element_type=f32)
        proj[:, lanes] = part
        total = total + jnp.sum(part * part, axis=-1, keepdims=True)
    scale = lax.rsqrt(total / branch.shape[1] + norm_eps)
    mixed[...] = (proj[:, : branch.shape[1]] * scale * group_gain[...]).astype(bf16)

    def forward(d):
        z_arrival(d).wait_recv()
        for t in range(1, n_tp):
            x_copy(d, t).start()

    def to_mate(d):
        for t in range(1, n_tp):
            x_arrival(d, t).wait_recv()
        p_copy(d).start()

    if nz > 1:
        forward(1)
    own_copy.wait()
    own_w.wait()
    own_ow.wait()
    for d in range(1, n_ep):
        w_arrival(d).wait_recv()
    for load in loads[:2]:
        load.wait()

    chunk = 16

    def normed(block, at):
        def one(i, _):
            r = pl.ds(pl.multiple_of(i * chunk, chunk), chunk)
            v = xg[block, r, :].astype(f32)
            out = pl.ds(pl.multiple_of(at + i * chunk, chunk), chunk)
            xn[out, :] = rms_scale(v, ffn_gain[...]).astype(bf16)
            return 0

        lax.fori_loop(0, rows // chunk, one, 0)

    diagonal = lax.broadcasted_iota(jnp.int32, (rows, rows), 0) == lax.broadcasted_iota(
        jnp.int32, (rows, rows), 1
    )

    def row_weights(block):
        line = wg[block, pl.ds(e, 1), :]
        return jnp.sum(jnp.where(diagonal, line, 0.0), axis=1, keepdims=True)

    step_f = min(256, gate.shape[1])

    def hidden_part():
        def one(n, _):
            span = pl.ds(pl.multiple_of(n * step_f, step_f), step_f)
            g = jnp.dot(xn[...], gate[:, span], preferred_element_type=f32)
            u = jnp.dot(xn[...], up[:, span], preferred_element_type=f32)
            g = jnp.minimum(g, clamp_limit)
            u = jnp.clip(u, -clamp_limit, clamp_limit)
            hid[:, span] = ((u + 1.0) * g * jax.nn.sigmoid(sigmoid_slope * g)).astype(bf16)
            return 0

        lax.fori_loop(0, gate.shape[1] // step_f, one, 0)

    step_d = min(256, width)

    def down_part(s):
        mine = row_weights(src_ep(s))
        theirs = row_weights(src_mate(s))

        def one(q, _):
            span = pl.ds(pl.multiple_of(q * step_d, step_d), step_d)
            y = jnp.dot(hid[...], down[:, span], preferred_element_type=f32)
            pown[s % 2, :, span] = y[:rows] * mine
            psend[s, :, span] = (y[rows:] * theirs).astype(bf16)
            return 0

        lax.fori_loop(0, width // step_d, one, 0)

    def mate_sum(s):
        return remote(psend.at[s], precv.at[s], s_ps.at[s], r_ps.at[s], mate, j)

    def t_copy(s, t):
        return remote(
            tsend.at[s, :, colsl(tp_at(t))], trecv.at[s, t], s_t.at[s, t], r_t.at[s, t], e, tp_at(t)
        )

    def f_copy(s):
        return remote(fsend.at[s], frecv.at[s], s_f.at[s], r_f.at[s], src_ep(s), j)

    def stage_two(s):
        mate_sum(s).wait_recv()

        def one(i, _):
            r = pl.ds(pl.multiple_of(i * chunk, chunk), chunk)
            tsend[s, r, :] = (pown[s % 2, r, :] + precv[s, r, :].astype(f32)).astype(bf16)
            return 0

        lax.fori_loop(0, rows // chunk, one, 0)
        for t in range(1, n_tp):
            t_copy(s, t).start()

    def stage_three(s):
        for t in range(1, n_tp):
            t_copy(s, t).wait_recv()
        acc = tsend[s, :, colsl(j)].astype(f32)
        for t in range(1, n_tp):
            acc = acc + trecv[s, t].astype(f32)

        @pl.when(s == 0)
        def _():
            facc[...] = acc

        @pl.when(s > 0)
        def _():
            fsend[s] = acc.astype(bf16)
            f_copy(s).start()

    def project():
        for t in range(1, n_tp):
            owp_arrival(t).wait_recv()

        def one(q, total):
            part = jnp.dot(mixed[...], ow[q], preferred_element_type=f32)
            proj[:, colsl(q)] = part
            return total + jnp.sum(part * part, axis=-1, keepdims=True)

        total = lax.fori_loop(0, n_tp, one, jnp.zeros((branch_rows, 1), f32))
        scale = lax.rsqrt(total / width + norm_eps)

        def two(q, _):
            mixer_out[:, colsl(q)] = (proj[:, colsl(q)] * scale * out_gain[:, colsl(q)]).astype(bf16)
            return 0

        lax.fori_loop(0, n_tp, two, 0)

    def step(s, _):
        @pl.when(s < nz)
        def _():
            @pl.when(s == 0)
            def _():
                own_arr = remote(x_own, xg.at[mate], s_p.at[0], r_p.at[0], mate, j)
                own_arr.wait_recv()

            @pl.when(s > 0)
            def _():
                p_arrival(s).wait_recv()

            @pl.when(s + 2 < nz)
            def _():
                forward(s + 2)

            normed(src_ep(s), 0)
            normed(src_mate(s), rows)
            hidden_part()

        @pl.when((s > 0) & (s <= nz))
        def _():
            stage_two(s - 1)

        @pl.when(s < nz)
        def _():
            @pl.when(s == 0)
            def _():
                loads[2].wait()

            down_part(s)
            mate_sum(s).start()

            @pl.when(s + 1 < nz)
            def _():
                to_mate(s + 1)

        @pl.when(s == 0)
        def _():
            for t in range(1, n_tp):
                ow_arrival(t).wait_recv()
                owp_copy(t).start()

        @pl.when(s == nz)
        def _():
            project()

        @pl.when(s > 1)
        def _():
            stage_three(s - 2)

        return 0

    lax.fori_loop(0, nz + 2, step, 0)

    acc = facc[...]
    for d in range(1, nz):
        f_copy(d).wait_recv()
        acc = acc + frecv[d].astype(f32)
    expert_out[...] = acc.astype(bf16)

    own_p.wait_send()
    rim_copy.wait_send()
    for d in range(1, n_ep):
        w_copy(d).wait_send()
    for t in range(1, n_tp):
        ow_copy(t).wait_send()
        owp_copy(t).wait_send()

    def drain(s, _):
        mate_sum(s).wait_send()
        for t in range(1, n_tp):
            t_copy(s, t).wait_send()

        @pl.when(s > 0)
        def _():
            z_copy(s).wait_send()
            p_copy(s).wait_send()
            f_copy(s).wait_send()
            for t in range(1, n_tp):
                x_copy(s, t).wait_send()

        return 0

    lax.fori_loop(0, nz, drain, 0)


def per_device(
    n_ep, n_tp,
    branch_in, pool_weight, group_gain, out_weight, out_gain,
    ffn_input, ffn_gain, routes, route_weight, gate_weight, up_weight, down_weight,
):
    rows, width = ffn_input.shape
    nz = n_ep // 2
    cols = width // n_tp
    hidden = gate_weight.shape[2]
    branch_rows, branch_width = branch_in.shape
    named = routes[None, :, :] == jnp.arange(n_ep, dtype=jnp.int32)[:, None, None]
    w_own = jnp.sum(jnp.where(named, route_weight[None, :, :], 0.0), axis=2)
    vm = pl.BlockSpec(memory_space=pltpu.VMEM)
    anyspace = pl.BlockSpec(memory_space=pl.ANY)
    dma = pltpu.SemaphoreType.DMA
    return pl.pallas_call(
        functools.partial(kernel, n_ep, n_tp),
        out_shape=(
            jax.ShapeDtypeStruct((branch_rows, width), bf16),
            jax.ShapeDtypeStruct((rows, cols), bf16),
        ),
        in_specs=[vm] * 8 + [anyspace] * 3,
        out_specs=(vm, vm),
        scratch_shapes=[
            pltpu.VMEM((width, hidden), bf16),
            pltpu.VMEM((width, hidden), bf16),
            pltpu.VMEM((hidden, width), bf16),
            pltpu.VMEM((n_ep, rows, width), bf16),
            pltpu.VMEM((n_ep, n_ep, rows), f32),
            pltpu.VMEM((rim_rows, branch_width), bf16),
            pltpu.VMEM((n_tp, branch_width, cols), bf16),
            pltpu.VMEM((2 * rows, width), bf16),
            pltpu.VMEM((2 * rows, hidden), bf16),
            pltpu.VMEM((branch_rows, branch_width), bf16),
            pltpu.VMEM((branch_rows, width), f32),
            pltpu.VMEM((2, rows, width), f32),
            pltpu.VMEM((nz, rows, width), bf16),
            pltpu.VMEM((nz, rows, width), bf16),
            pltpu.VMEM((nz, rows, width), bf16),
            pltpu.VMEM((nz, n_tp, rows, cols), bf16),
            pltpu.VMEM((nz, rows, cols), bf16),
            pltpu.VMEM((nz, rows, cols), bf16),
            pltpu.VMEM((rows, cols), f32),
            dma((6,)),
            dma((nz,)), dma((nz,)),
            dma((nz, n_tp)), dma((nz, n_tp)),
            dma((nz,)), dma((nz,)),
            dma((n_ep,)), dma((n_ep,)),
            dma, dma,
            dma((n_tp,)), dma((n_tp,)),
            dma((n_tp,)), dma((n_tp,)),
            dma((nz,)), dma((nz,)),
            dma((nz, n_tp)), dma((nz, n_tp)),
            dma((nz,)), dma((nz,)),
        ],
        compiler_params=pltpu.CompilerParams(
            collective_id=0, has_side_effects=True, vmem_limit_bytes=67043328
        ),
    )(
        branch_in, pool_weight, group_gain.reshape(1, -1), out_weight, out_gain.reshape(1, -1),
        ffn_input, ffn_gain.reshape(1, -1), w_own, gate_weight, up_weight, down_weight,
    )


def solution(mesh):
    in_specs = (
        P(("ep", "tp"), None),
        P(),
        P(),
        P(None, "tp"),
        P(),
        P("ep", None),
        P(),
        P("ep", None),
        P("ep", None),
        P("ep", None, "tp"),
        P("ep", None, "tp"),
        P("ep", "tp", None),
    )
    out_specs = (P(("ep", "tp"), None), P("ep", "tp"))
    return jax.shard_map(
        functools.partial(per_device, mesh.shape["ep"], mesh.shape["tp"]),
        mesh=mesh, in_specs=in_specs, out_specs=out_specs, check_vma=False,
    )
```

time: 231 us -> 83.5 us (0.36)
  waiting for transfers between devices: 130 us -> 0 us
  Pallas kernels: 0 us -> 77.5 us
  blocking collectives: 32.8 us -> 0 us
  matrix products: 22.7 us -> 0 us
  between operations: 14 us -> 0.64 us
  local copies, waits for them, and re-layouts: 15 us -> 3.87 us
  starting transfers between devices: 8.11 us -> 0 us
  other arithmetic: 7.78 us -> 1.3 us
    all_gather x2 -> x0, waiting for transfers between devices: 83.2 us -> none  [the longest x1 51.6 us: per_device(): lax.all_gather(arrived, 'tp', axis=0, tiled=True)]
    pallas_call x0 -> x1, Pallas kernels: none -> 77.5 us  [per_device(): pl.pallas_call(functools.partial(kernel, n_ep, n_tp), out_shape=(jax.Shap...]
    reduce_scatter x1 -> x0, waiting for transfers between devices: 45.5 us -> none  [send_home(): lax.psum_scatter(partial_sum.astype(jnp.bfloat16), 'tp', scatter_dimensio...]
    all_to_all x1 -> x0, blocking collectives: 32.8 us -> none  [per_device(): lax.all_to_all(my_share, 'ep', split_axis=1, concat_axis=1, tiled=True)]
    dot_general x8 -> x0, matrix products: 22.7 us -> none  [the longest x1 7.64 us: expert_hidden(): jnp.einsum('sed,df->sef', slot_rows, gate_local, preferred_element_type=j...]
    gather x2 -> x0, local copies, waits for them, and re-layouts: 7.99 us -> none  [the longest x1 6.02 us: per_device(): slot_rows = padded[owner_rows].reshape(capacity, expert_count, model_width)]
    all_to_all x1 -> x0, starting transfers between devices: 4.62 us -> none  [send_home(): return lax.all_to_all(summed, 'ep', split_axis=1, concat_axis=1, tiled=True)]
    convert_element_type x5 -> x0, other arithmetic: 3.68 us -> none  [the longest x1 1.24 us: per_device(): rms_scale(ffn_input.astype(jnp.float32), ffn_gain).astype(jnp.bfloat16)]
  transfers between devices with their start and end apart: 5 -> 0, of which waited for: 4 -> 0; matrix products, arithmetic and copies ran while one was open for 3% -> 0% of each run, Pallas kernels for 0% -> 0%
where the time goes in v1:
time: 83.5 us; the launch traced here: 83.3 us
  Pallas kernels  77.5 us (93%)
  local copies, waits for them, and re-layouts  3.87 us (5%)
  other arithmetic  1.3 us (2%)
    pallas_call x1, Pallas kernels, per_device(): pl.pallas_call(functools.partial(kernel, n_ep, n_tp), out_shape=(jax.Shap...  77.5 us
    unnamed x2, local copies, waits for them, and re-layouts  3.87 us

profile of v1, /device:TPU:0, one launch (start us, length us, event | category | flops | bytes accessed | tf_op | source)
XLA Modules:
  0.0 83.3 jit_solution(18375137492544076625)
XLA Ops:
  0.6 1.3 %select_reduce_fusion.w_own = f32[8,128]{1,0:T(8,128)} fusion(f32[128,4]{0,1:T(4,128)} %param.20, s32[128,4]{0,1:T(4,128)} %param.19), kind=kLoop, calls=%fused_computation | loop fusion | flops 11264 | bytes 8192 | tf_op jit(solution)/shard_map/reduce_sum | solution.py:402
  1.9 77.5 %shard_map.131 = (bf16[256,2048]{1,0:T(8,128)(2,1)}, bf16[128,512]{1,0:T(8,128)(2,1)}) custom-call(bf16[256,512]{1,0:T(8,128)(2,1)} %branch.1, bf16[4,128,128]{2,1,0:T(8,128)(2,1)} %pool_w.1, f32[1,512]{1,0:T(1,128)} %bitcast.5, bf16[512,512]{1,0:T(8,128)(2,1)} %out_w.1, f32[1,2048]{1,0:T(1,128)} %bitcast.3, bf16[128,2048]{1,0:T(8,128)(2,1)} %x_own.1, ...), custom_call_target="tpu_custom_call" | custom-call | tf_op jit(solution)/shard_map/pallas_call | solution.py:406
  79.4 2.3 %copy.18 = bf16[256,2048]{1,0:T(8,128)(2,1)} copy(bf16[256,2048]{1,0:T(8,128)(2,1)} %get-tuple-element.4) | data formatting | bytes 2097152
  81.7 1.6 %copy.19 = bf16[128,512]{1,0:T(8,128)(2,1)} copy(bf16[128,512]{1,0:T(8,128)(2,1)} %get-tuple-element.5) | data formatting | bytes 262144

commit v2 on v1

--- a/solution.py
+++ b/solution.py
@@ -24,7 +24,7 @@
     n_ep, n_tp,
     branch, pool_w, group_gain, out_w, out_gain, x_own, ffn_gain, w_own, gate_h, up_h, down_h,
     mixer_out, expert_out,
-    gate, up, down, xg, wg, rim, ow, xn, hid, mixed, proj,
+    gate, up, down, xg, wg, rim, ow, hid, mixed, proj,
     pown, psend, precv, tsend, trecv, fsend, frecv, facc,
     local_sem, s_z, r_z, s_x, r_x, s_p, r_p, s_w, r_w, s_rim, r_rim,
     s_ow, r_ow, s_owp, r_owp, s_ps, r_ps, s_t, r_t, s_f, r_f,
@@ -68,10 +68,8 @@
         pltpu.make_async_copy(up_h.at[0], up, local_sem.at[1]),
         pltpu.make_async_copy(down_h.at[0], down, local_sem.at[2]),
     ]
-    own_copy = pltpu.make_async_copy(x_own, xg.at[e], local_sem.at[3])
     own_w = pltpu.make_async_copy(w_own, wg.at[e], local_sem.at[4])
     own_ow = pltpu.make_async_copy(out_w, ow.at[j], local_sem.at[5])
-    own_copy.start()
     own_w.start()
     own_ow.start()
     for load in loads:
@@ -84,11 +82,20 @@
         pl.semaphore_signal(barrier, inc=1, device_id=(e, tp_at(t)), device_id_type=MESH)
     pl.semaphore_signal(barrier, inc=1, device_id=nxt, device_id_type=MESH)
     pl.semaphore_signal(barrier, inc=1, device_id=prv, device_id_type=MESH)
+
+    chunk = 16
+
+    def norm_rows(i, _):
+        r = pl.ds(pl.multiple_of(i * chunk, chunk), chunk)
+        xg[e, r, :] = rms_scale(x_own[r, :].astype(f32), ffn_gain[...]).astype(bf16)
+        return 0
+
+    lax.fori_loop(0, rows // chunk, norm_rows, 0)
     pl.semaphore_wait(barrier, n_ep - 1 + n_tp - 1 + 2)
 
     def z_copy(d):
         return remote(
-            x_own.at[:, colsl(j)], xg.at[e, :, colsl(j)], s_z.at[d], r_z.at[d], ep_at(d), j
+            xg.at[e, :, colsl(j)], xg.at[e, :, colsl(j)], s_z.at[d], r_z.at[d], ep_at(d), j
         )
 
     def z_arrival(d):
@@ -111,7 +118,7 @@
         view = xg.at[src_mate(d)]
         return remote(view, view, s_p.at[d], r_p.at[d], mate, j)
 
-    own_p = remote(x_own, xg.at[e], s_p.at[0], r_p.at[0], mate, j)
+    own_p = remote(xg.at[e], xg.at[e], s_p.at[0], r_p.at[0], mate, j)
     half = out_w.shape[0] // 2
     my_half = pl.ds(pl.multiple_of(c * half, half), half)
     mate_half = pl.ds(pl.multiple_of((1 - c) * half, half), half)
@@ -187,7 +194,6 @@
 
     if nz > 1:
         forward(1)
-    own_copy.wait()
     own_w.wait()
     own_ow.wait()
     for d in range(1, n_ep):
@@ -195,18 +201,6 @@
     for load in loads[:2]:
         load.wait()
 
-    chunk = 16
-
-    def normed(block, at):
-        def one(i, _):
-            r = pl.ds(pl.multiple_of(i * chunk, chunk), chunk)
-            v = xg[block, r, :].astype(f32)
-            out = pl.ds(pl.multiple_of(at + i * chunk, chunk), chunk)
-            xn[out, :] = rms_scale(v, ffn_gain[...]).astype(bf16)
-            return 0
-
-        lax.fori_loop(0, rows // chunk, one, 0)
-
     diagonal = lax.broadcasted_iota(jnp.int32, (rows, rows), 0) == lax.broadcasted_iota(
         jnp.int32, (rows, rows), 1
     )
@@ -215,13 +209,14 @@
         line = wg[block, pl.ds(e, 1), :]
         return jnp.sum(jnp.where(diagonal, line, 0.0), axis=1, keepdims=True)
 
-    step_f = min(256, gate.shape[1])
-
-    def hidden_part():
+    step_f = min(512, gate.shape[1])
+
+    def hidden_part(s):
         def one(n, _):
             span = pl.ds(pl.multiple_of(n * step_f, step_f), step_f)
-            g = jnp.dot(xn[...], gate[:, span], preferred_element_type=f32)
-            u = jnp.dot(xn[...], up[:, span], preferred_element_type=f32)
+            both = jnp.concatenate([xg[src_ep(s)], xg[src_mate(s)]], axis=0)
+            g = jnp.dot(both, gate[:, span], preferred_element_type=f32)
+            u = jnp.dot(both, up[:, span], preferred_element_type=f32)
             g = jnp.minimum(g, clamp_limit)
             u = jnp.clip(u, -clamp_limit, clamp_limit)
             hid[:, span] = ((u + 1.0) * g * jax.nn.sigmoid(sigmoid_slope * g)).astype(bf16)
@@ -229,7 +224,7 @@
 
         lax.fori_loop(0, gate.shape[1] // step_f, one, 0)
 
-    step_d = min(256, width)
+    step_d = min(512, width)
 
     def down_part(s):
         mine = row_weights(src_ep(s))
@@ -306,7 +301,7 @@
         def _():
             @pl.when(s == 0)
             def _():
-                own_arr = remote(x_own, xg.at[mate], s_p.at[0], r_p.at[0], mate, j)
+                own_arr = remote(xg.at[mate], xg.at[mate], s_p.at[0], r_p.at[0], mate, j)
                 own_arr.wait_recv()
 
             @pl.when(s > 0)
@@ -317,9 +312,7 @@
             def _():
                 forward(s + 2)
 
-            normed(src_ep(s), 0)
-            normed(src_mate(s), rows)
-            hidden_part()
+            hidden_part(s)
 
         @pl.when((s > 0) & (s <= nz))
         def _():
@@ -419,7 +412,6 @@
             pltpu.VMEM((n_ep, n_ep, rows), f32),
             pltpu.VMEM((rim_rows, branch_width), bf16),
             pltpu.VMEM((n_tp, branch_width, cols), bf16),
-            pltpu.VMEM((2 * rows, width), bf16),
             pltpu.VMEM((2 * rows, hidden), bf16),
             pltpu.VMEM((branch_rows, branch_width), bf16),
             pltpu.VMEM((branch_rows, width), f32),

time: 83.5 us -> 73.2 us (0.88)
  Pallas kernels: 77.5 us -> 67.1 us
    pallas_call x1, Pallas kernels: 77.5 us -> 67.1 us  [per_device(): pl.pallas_call(functools.partial(kernel, n_ep, n_tp), out_shape=(jax.Shap...]
where the time goes in v2:
time: 73.2 us; the launch traced here: 72.9 us
  Pallas kernels  67.1 us (92%)
  local copies, waits for them, and re-layouts  3.87 us (5%)
  other arithmetic  1.3 us (2%)
    pallas_call x1, Pallas kernels, per_device(): pl.pallas_call(functools.partial(kernel, n_ep, n_tp), out_shape=(jax.Shap...  67.1 us
    unnamed x2, local copies, waits for them, and re-layouts  3.87 us

profile of v2, /device:TPU:0, one launch (start us, length us, event | category | flops | bytes accessed | tf_op | source)
XLA Modules:
  0.0 72.9 jit_solution(12522479872014948391)
XLA Ops:
  0.6 1.3 %select_reduce_fusion.w_own = f32[8,128]{1,0:T(8,128)} fusion(f32[128,4]{0,1:T(4,128)} %param.20, s32[128,4]{0,1:T(4,128)} %param.19), kind=kLoop, calls=%fused_computation | loop fusion | flops 11264 | bytes 8192 | tf_op jit(solution)/shard_map/reduce_sum | solution.py:395
  1.9 67.1 %shard_map.131 = (bf16[256,2048]{1,0:T(8,128)(2,1)}, bf16[128,512]{1,0:T(8,128)(2,1)}) custom-call(bf16[256,512]{1,0:T(8,128)(2,1)} %branch.1, bf16[4,128,128]{2,1,0:T(8,128)(2,1)} %pool_w.1, f32[1,512]{1,0:T(1,128)} %bitcast.5, bf16[512,512]{1,0:T(8,128)(2,1)} %out_w.1, f32[1,2048]{1,0:T(1,128)} %bitcast.3, bf16[128,2048]{1,0:T(8,128)(2,1)} %x_own.1, ...), custom_call_target="tpu_custom_call" | custom-call | tf_op jit(solution)/shard_map/pallas_call | solution.py:399
  69.1 2.3 %copy.18 = bf16[256,2048]{1,0:T(8,128)(2,1)} copy(bf16[256,2048]{1,0:T(8,128)(2,1)} %get-tuple-element.4) | data formatting | bytes 2097152
  71.4 1.6 %copy.19 = bf16[128,512]{1,0:T(8,128)(2,1)} copy(bf16[128,512]{1,0:T(8,128)(2,1)} %get-tuple-element.5) | data formatting | bytes 262144
